TPU v7x, 768 devices: a whole 4x8x12 slice. The times are simulated.
768 devices in a mesh: ep: 24 (over z, core), tp: 32 (over y, x).
Axes of the slice: x: 4, y: 8, z: 12, core: 2. Of those that a mesh axis runs over, the one named last changes fastest.
Arguments:
- tokens: bfloat16 [3072, 2048], P('ep', 'tp'), may hold values from -6 to 6
- routes: int32 [3072, 2], P('ep'), may hold values from 0 to 23, as said below
- route_weights: float32 [3072, 2], P('ep'), may hold values from 0.1 to 1
- grad_out: bfloat16 [3072, 2048], P('ep', 'tp'), may hold values from -6 to 6
- w_gate: bfloat16 [24, 2048, 2048], P('ep', 'tp'), may hold values from -0.125 to 0.125
- w_up: bfloat16 [24, 2048, 2048], P('ep', 'tp'), may hold values from -0.125 to 0.125
- w_down: bfloat16 [24, 2048, 2048], P('ep', 'tp')
Outputs:
- grad_tokens: bfloat16 [3072, 2048], P('ep', 'tp')
- grad_route: float32 [3072, 2], P('ep')
- grad_gate: float32 [24, 2048, 2048], P('ep', 'tp')
- grad_up: float32 [24, 2048, 2048], P('ep', 'tp')
- grad_down: float32 [24, 2048, 2048], P('ep', 'tp')
- gate_row_norms: float32 [24, 2048], P('ep')
- up_row_norms: float32 [24, 2048], P('ep')
- down_row_norms: float32 [24, 2048], P('ep', 'tp')
Inputs may be any that keep to these rules, and one draw needn't show every extreme that they name: `routes`: each token names two different experts of one group: group g holds experts g * 4 to g * 4 + 3. Among the 128 rows of one device along ep no expert is named more than 16 times, and in every draw some expert is named exactly 16 times by the rows of every device along ep.
All inputs are finite; a program needn't handle non-finite values.
Results may differ from a plain program's by a relative error of at most 0.017.
Values may be sent and summed in bfloat16 or wider, within the bound.
No kernel may reach another device: no remote copies, remote signals or barrier semaphores. Data moves between devices by JAX's collectives and lax.ppermute only.
A program may use at most 64 MiB of HBM per device.

v0:
```python
import jax
import jax.numpy as jnp
from jax import lax
from jax.experimental import pallas as pl
from jax.experimental.pallas import tpu as pltpu
from jax.sharding import Mesh
from jax.sharding import PartitionSpec as P


SLOTS = 16
HALF = 64
ROOM = 20 * 2**20
F32 = jnp.float32
BF16 = jnp.bfloat16


def dot(a, b, ca, cb):
    return lax.dot_general(a, b, (((ca,), (cb,)), ((), ())), preferred_element_type=F32)


def split_hi_lo(v):
    hi = v.astype(BF16)
    return hi, (v - hi.astype(F32)).astype(BF16)


def placed(routes, tokens, experts):
    ids = lax.broadcasted_iota(jnp.int32, (experts, tokens), 0)
    first = ids == routes[0:1, :]
    second = ids == routes[1:2, :]
    named = (first | second).astype(F32).astype(BF16)
    before = (
        lax.broadcasted_iota(jnp.int32, (tokens, tokens), 0)
        < lax.broadcasted_iota(jnp.int32, (tokens, tokens), 1)
    ).astype(F32).astype(BF16)
    rank = dot(named, before, 1, 0) + (ids * SLOTS).astype(F32)
    return [
        jnp.sum(jnp.where(m, rank, 0.0), axis=0, keepdims=True).astype(jnp.int32)
        for m in (first, second)
    ]


def chosen(position, slots):
    at = lax.broadcasted_iota(jnp.int32, (slots, position.shape[1]), 0)
    return (at == position).astype(F32).astype(BF16)


def fetched(sources, targets, sems):
    copies = [
        pltpu.make_async_copy(a, b, sems.at[k]) for k, (a, b) in enumerate(zip(sources, targets))
    ]
    for c in copies:
        c.start()
    return copies


def dispatch_body(
    tokens_far,
    routes_far,
    weights_far,
    cotangent_far,
    gate_far,
    up_far,
    down_far,
    sent,
    positions,
    weights,
    w_gate,
    w_up,
    w_down,
    tokens,
    routes,
    cotangent,
    sems,
    later_sems,
):
    far = (tokens_far, routes_far, weights_far, cotangent_far)
    now = fetched(far, (tokens, routes, weights, cotangent), sems)
    later = fetched((gate_far, up_far, down_far), (w_gate, w_up, w_down), later_sems)
    for c in now:
        c.wait()
    _, count = tokens.shape
    slots = sent.shape[0]
    at = placed(routes[...], count, slots // SLOTS)
    positions[...] = jnp.concatenate(at, axis=0)
    x = tokens[...]
    g = cotangent[...].astype(F32)
    scaled = [(g * weights[k : k + 1, :]).astype(BF16) for k in range(2)]
    rows = jnp.concatenate(
        [jnp.concatenate([x, x], axis=1), jnp.concatenate(scaled, axis=1)], axis=0
    )
    pick = jnp.concatenate([chosen(p, slots) for p in at], axis=1)
    sent[...] = dot(pick, rows, 1, 1).astype(BF16)
    for c in later:
        c.wait()


def quarter_weights_body(here, w_gate, w_up, w_down, o0, o1, o2, o3):
    outs = (o0, o1, o2, o3)
    nx = len(outs)
    hid = w_gate.shape[0]

    def write(at):
        for m, w in enumerate((w_gate, w_up, w_down)):
            for d, out in enumerate(outs):
                q = (at + d) % nx
                for j in range(out.shape[1] // 128):
                    a, b = ((2 * j) * nx + q) * HALF, ((2 * j + 1) * nx + q) * HALF
                    out[m * hid : (m + 1) * hid, j * 128 : (j + 1) * 128] = jnp.concatenate(
                        [w[:, a : a + HALF], w[:, b : b + HALF]], axis=1
                    )

    for at in range(nx):
        pl.when(here[0] == at)(lambda at=at: write(at))


def partial_body(here, rows, w0, w1, w2, w3, out, x_out, s_out):
    weights = (w0, w1, w2, w3)
    nx = len(weights)
    ny = rows.shape[0]
    for j in range(ny // 2):
        a, b = rows[2 * j], rows[2 * j + 1]
        x_out[:, j * 128 : (j + 1) * 128] = jnp.concatenate([a[:, :HALF], b[:, :HALF]], axis=1)
        s_out[:, j * 128 : (j + 1) * 128] = jnp.concatenate([a[:, HALF:], b[:, HALF:]], axis=1)
    x, s = x_out[...], s_out[...]
    hid = w0.shape[0] // 3
    both = dot(jnp.concatenate([w[: 2 * hid, :] for w in weights], axis=0), x, 1, 1)
    down = dot(jnp.concatenate([w[2 * hid :, :] for w in weights], axis=0), s, 1, 1)
    for d in range(nx):
        q = (here[0] + nx - d) % nx
        out[q, : 2 * hid, :] = both[2 * d * hid : 2 * (d + 1) * hid].astype(BF16)
        out[q, 2 * hid :, :] = down[d * hid : (d + 1) * hid].astype(BF16)


def activation_body(parts, out):
    total = parts[0].astype(F32)
    for q in range(1, parts.shape[0]):
        total = total + parts[q].astype(F32)
    hid = total.shape[0] // 3
    gate, up, dhid = total[:hid], total[hid : 2 * hid], total[2 * hid :]
    sig = 1.0 / (1.0 + jnp.exp(-gate))
    active = gate * sig
    slope = sig * (1.0 + gate * (1.0 - sig))
    hidden = (active * up).astype(BF16)
    dgate = (dhid * up * slope).astype(BF16)
    dup = (dhid * active).astype(BF16)
    value = jnp.sum(hidden.astype(F32) * dhid, axis=0, keepdims=True)
    hi, lo = split_hi_lo(value)
    pad = jnp.zeros((out.shape[1] - 3 * hid - 2, out.shape[2]), BF16)
    block = jnp.concatenate([dgate, dup, hidden, hi, lo, pad], axis=0)
    for q in range(out.shape[0]):
        out[q] = block


def backward_body(here, acts, w0, w1, w2, w3, x_rows, s_rows, back, *grads):
    weights = (w0, w1, w2, w3)
    nx, ny = len(weights), back.shape[0]
    hid = w0.shape[0] // 3
    width = w0.shape[1]
    slots = acts.shape[2]
    pairs = [acts[(here[0] + d) % nx, : 2 * hid, :] for d in range(nx)]
    terms = dot(
        jnp.concatenate([w[: 2 * hid, :] for w in weights], axis=0),
        jnp.concatenate([pairs[0]] + pairs[:0:-1], axis=0),
        0,
        0,
    ).astype(BF16)
    hiddens = [acts[(here[0] + d) % nx, 2 * hid : 3 * hid, :] for d in range(nx)]
    pair = dot(jnp.concatenate(pairs, axis=0), x_rows[...], 1, 0)
    down = dot(jnp.concatenate(hiddens, axis=0), s_rows[...], 1, 0)
    norms = [jnp.zeros((1, width), F32) for _ in range(2)]
    value = jnp.zeros((1, slots), F32)
    for d in range(nx):
        grads[d][: 2 * hid, :] = pair[2 * d * hid : 2 * (d + 1) * hid].astype(BF16)
        grads[d][2 * hid :, :] = down[d * hid : (d + 1) * hid].astype(BF16)
        for m in range(2):
            part = pair[(2 * d + m) * hid : (2 * d + m + 1) * hid]
            norms[m] = norms[m] + jnp.sum(part * part, axis=0, keepdims=True)
        tail = acts[(here[0] + d) % nx, 3 * hid : 3 * hid + 2, :].astype(F32)
        value = value + tail[0:1] + tail[1:2]
    flat = [v for n in norms for v in split_hi_lo(n)]
    lines = list(split_hi_lo(value))
    spare = (back.shape[1] - HALF - len(lines)) * slots - len(flat) * width
    flat = jnp.concatenate(flat + [jnp.zeros((1, spare), BF16)], axis=1)
    lines += [flat[:, k : k + slots] for k in range(0, flat.shape[1], slots)]
    extra = jnp.concatenate(lines, axis=0)
    for j in range(ny):
        back[j, :HALF, :] = terms[j * HALF : (j + 1) * HALF]
        back[j, HALF:, :] = extra


def gathered_body(parts, sent, norms):
    total = parts[0].astype(F32)
    for j in range(1, parts.shape[0]):
        total = total + parts[j].astype(F32)
    slots = total.shape[1]
    hi, lo = split_hi_lo(total[HALF : HALF + 1] + total[HALF + 1 : HALF + 2])
    pad = jnp.zeros((128 - HALF - 2, slots), F32)
    block = jnp.concatenate([total[:HALF], hi.astype(F32), lo.astype(F32), pad], axis=0)
    sent[...] = block.T.astype(BF16)
    flat = jnp.concatenate([total[k : k + 1] for k in range(HALF + 2, total.shape[0])], axis=1)
    tiles = [flat[:, k : k + 128] for k in range(0, flat.shape[1], 128)]
    each = norms.shape[0] // 2
    lines = [
        tiles[2 * m * each + k] + tiles[(2 * m + 1) * each + k]
        for m in range(2)
        for k in range(each)
    ]
    norms[...] = jnp.concatenate(lines, axis=0)


def halves(parts, lines, y, h):
    at = (y * HALF) % parts.shape[2]
    pair = [parts[2 * h + k, lines, at : at + HALF] for k in range(2)]
    return jnp.concatenate(pair, axis=1).astype(F32)


def grads_body(here, p0, p1, p2, p3, grad_gate, grad_up, grad_down, down_norms, parts):
    received = (p0, p1, p2, p3)
    nx = len(received)
    hid = grad_gate.shape[0]
    for d, p in enumerate(received):
        parts[(here[0] + nx - d) % nx] = p[...]
    acc = jnp.zeros((hid, 128), F32)
    for m, out in enumerate((grad_gate, grad_up, grad_down)):
        for y in range(parts.shape[2] // HALF):
            for h in range(nx // 2):
                tile = halves(parts, slice(m * hid, (m + 1) * hid), y, h)
                at = (y * (nx // 2) + h) * 128
                out[:, at : at + 128] = tile
                if m == 2:
                    acc = acc + tile * tile
    down_norms[...] = jnp.sum(acc.T, axis=0, keepdims=True)


def combine_body(
    here,
    back,
    positions,
    weights,
    n0,
    n1,
    n2,
    n3,
    grad_tokens,
    grad_route,
    gate_norms,
    up_norms,
    parts,
):
    slots, count = back.shape[0], positions.shape[1]
    pick = jnp.concatenate([chosen(positions[k : k + 1, :], slots) for k in range(2)], axis=1)
    got = dot(back[...], pick, 0, 0)
    grad_tokens[...] = (got[:HALF, :count] + got[:HALF, count:]).astype(BF16)
    value = got[HALF : HALF + 1] + got[HALF + 1 : HALF + 2]
    value = jnp.concatenate([value[:, :count], value[:, count:]], axis=0)
    grad_route[...] = value / weights[...]
    nx = parts.shape[0]
    each = parts.shape[1] // 2
    for d, n in enumerate((n0, n1, n2, n3)):
        parts[(here[0] + nx - d) % nx] = n[...]
    for m, out in enumerate((gate_norms, up_norms)):
        out[...] = jnp.concatenate(
            [
                halves(parts, slice(m * each + y // 2, m * each + y // 2 + 1), y, h)
                for y in range(2 * each)
                for h in range(nx // 2)
            ],
            axis=0,
        )


def call(body, outs, *args, fetch=False, far=False, scratch=(), aliases=None):
    smem = pl.BlockSpec(memory_space=pltpu.SMEM)
    vmem = pl.BlockSpec(memory_space=pltpu.VMEM)
    space = pltpu.HBM if fetch else pltpu.VMEM
    specs = [smem if a.ndim == 1 else pl.BlockSpec(memory_space=space) for a in args]
    args = [a if a.ndim == 1 else pltpu.with_memory_space_constraint(a, space) for a in args]
    shape = jax.ShapeDtypeStruct if far else pltpu.VMEM
    return pl.pallas_call(
        body,
        out_shape=[shape(s, d) for s, d in outs],
        in_specs=specs,
        out_specs=[vmem] * len(outs),
        scratch_shapes=list(scratch),
        input_output_aliases=aliases or {},
        compiler_params=pltpu.CompilerParams(vmem_limit_bytes=ROOM),
    )(*args)


def swap(a, axis):
    return lax.all_to_all(a, axis, 0, 0, tiled=True)


def shifted(piece, axis, d):
    n = lax.axis_size(axis)
    return lax.ppermute(piece, axis, [(i, (i + d) % n) for i in range(n)])


def layer(tokens, routes, route_weights, grad_out, w_gate, w_up, w_down):
    ny, nx = lax.axis_size("y"), lax.axis_size("x")
    sources = lax.axis_size("z") * lax.axis_size("c")
    here = lax.axis_index("x").astype(jnp.int32).reshape(1)
    count, feat = tokens.shape
    _, hid, width = w_gate.shape
    slots = sources * SLOTS
    quarter = width // nx
    small = [tokens.T, routes.T, route_weights.T, grad_out.T]
    sent, positions, scales, *local = call(
        dispatch_body,
        [((slots, 2 * feat), BF16), ((2, count), jnp.int32), ((2, count), F32)]
        + [((hid, width), BF16)] * 3,
        *small,
        w_gate[0],
        w_up[0],
        w_down[0],
        fetch=True,
        scratch=[pltpu.VMEM(small[k].shape, small[k].dtype) for k in (0, 1, 3)]
        + [pltpu.SemaphoreType.DMA((4,)), pltpu.SemaphoreType.DMA((3,))],
    )
    w_sent = call(quarter_weights_body, [((3 * hid, quarter), BF16)] * nx, here, *local)
    mine = swap(sent.reshape(sources, SLOTS, 2 * feat), ("z", "c")).reshape(slots, 2 * feat)
    weights = [w_sent[0]] + [shifted(w_sent[d], "x", d) for d in range(1, nx)]
    rows = lax.all_gather(mine, "y", axis=0, tiled=False)
    parts, x_rows, s_rows = call(
        partial_body,
        [
            ((nx, 3 * hid, slots), BF16),
            ((slots, quarter), BF16),
            ((slots, quarter), BF16),
        ],
        here,
        rows,
        *weights,
    )
    parts = swap(parts, "x")
    (acts,) = call(activation_body, [((nx, 3 * hid + 8, slots), BF16)], parts)
    acts = swap(acts, "x")
    back, *grads = call(
        backward_body,
        [((ny, feat + 8, slots), BF16)]
        + [((3 * hid, quarter), BF16)] * nx,
        here,
        acts,
        *weights,
        x_rows,
        s_rows,
    )
    grads = [grads[0]] + [shifted(grads[d], "x", d) for d in range(1, nx)]
    back = swap(back, "y")
    back, *grads[1::2] = lax.optimization_barrier((back, *grads[1::2]))
    back_sent, norms = call(
        gathered_body, [((slots, 128), BF16), ((quarter // 64, 128), F32)], back
    )
    norms = [norms] + [shifted(norms, "x", d) for d in range(1, nx)]
    back = swap(back_sent.reshape(sources, SLOTS, 128), ("z", "c")).reshape(slots, 128)
    grad_gate, grad_up, grad_down, down_norms = call(
        grads_body,
        [((hid, width), F32)] * 3 + [((1, hid), F32)],
        here,
        *grads,
        far=True,
        scratch=[pltpu.VMEM((nx, 3 * hid, quarter), BF16)],
    )
    grad_tokens, grad_route, gate_norms, up_norms = call(
        combine_body,
        [((feat, count), BF16), ((2, count), F32)] + [((width // 128, 128), F32)] * 2,
        here,
        back,
        positions,
        scales,
        *norms,
        far=True,
        scratch=[pltpu.VMEM((nx, quarter // 64, 128), F32)],
    )
    return (
        grad_tokens.T,
        grad_route.T,
        grad_gate[None],
        grad_up[None],
        grad_down[None],
        gate_norms.reshape(1, width),
        up_norms.reshape(1, width),
        down_norms,
    )


def solution(mesh):
    ep, tp = ("z", "c"), ("y", "x")
    fine = Mesh(mesh.devices.reshape(12, 2, 8, 4), ep + tp)
    in_specs = (
        P(ep, tp),
        P(ep, None),
        P(ep, None),
        P(ep, tp),
        P(ep, tp, None),
        P(ep, tp, None),
        P(ep, tp, None),
    )
    out_specs = (
        P(ep, tp),
        P(ep, None),
        P(ep, tp, None),
        P(ep, tp, None),
        P(ep, tp, None),
        P(ep, None),
        P(ep, None),
        P(ep, tp),
    )
    return jax.shard_map(layer, mesh=fine, in_specs=in_specs, out_specs=out_specs, check_vma=False)
```

profile of v0, /device:TPU:1, one launch (start us, length us, event | category | flops | bytes accessed | tf_op | source)
XLA Modules:
  0.0 127.0 jit_solution(5598450025091781021)
XLA Ops:
  0.6 2.0 %shard_map.134 = (bf16[384,128]{1,0:T(8,128)(2,1)}, s32[2,128]{1,0:T(2,128)S(1)}, f32[2,128]{1,0:T(2,128)S(1)}, bf16[64,2048]{1,0:T(8,128)(2,1)S(1)}, bf16[64,20...) custom-call(bf16[64,128]{1,0:T(8,128)(2,1)} %bitcast.24, s32[2,128]{1,0:T(2,128)} %bitcast.26, f32[2,128]{1,0:T(2,128)} %bitcast.27, ...), custom_call_target="tpu_custom_call" | custom-call | tf_op jit(solution)/shard_map/pallas_call | solution.py:279
  2.6 16.7 %all-to-all-start = ((bf16[24,16,128]{2,1,0:T(8,128)(2,1)}), bf16[24,16,128]{2,1,0:T(8,128)(2,1)S(1)}, u32[]{:S(2)}, u32[]{:S(2)}) async-start(bf16[24,16,128]{2,1,0:T(8,128)(2,1)} %bitcast.8), calls=%async_computation | async-start | bytes 196608 | tf_op jit(solution)/shard_map/all_to_all | solution.py:291
  19.3 0.3 shard_map.135
  19.6 3.1 %collective-permute-start = (bf16[192,512]{1,0:T(8,128)(2,1)S(1)}, bf16[192,512]{1,0:T(8,128)(2,1)S(1)}, u32[]{:S(2)}, u32[]{:S(2)}) collective-permute-start(bf16[192,512]{1,0:T(8,128)(2,1)S(1)} %get-tuple-element.44), channel_id=1, source_target_pairs={{0,1},{1,2},{2,3},{3,0},{4,5},{5,6},{6,7},{7,4},{8,9},{9,10},{10,1... | collective-permute-start | bytes 589832 | tf_op jit(solution)/shard_map/ppermute | solution.py:296
  22.7 4.4 %collective-permute-start.1 = (bf16[192,512]{1,0:T(8,128)(2,1)S(1)}, bf16[192,512]{1,0:T(8,128)(2,1)S(1)}, u32[]{:S(2)}, u32[]{:S(2)}) collective-permute-start(bf16[192,512]{1,0:T(8,128)(2,1)S(1)} %get-tuple-element.45), channel_id=1, source_target_pairs={{0,2},{1,3},{2,0},{3,1},{4,6},{5,7},{6,4},{7,5},{8,10},{9,11},{10,... | collective-permute-start | bytes 589832 | tf_op jit(solution)/shard_map/ppermute | solution.py:296
  27.1 3.1 %collective-permute-start.2 = (bf16[192,512]{1,0:T(8,128)(2,1)S(1)}, bf16[192,512]{1,0:T(8,128)(2,1)S(1)}, u32[]{:S(2)}, u32[]{:S(2)}) collective-permute-start(bf16[192,512]{1,0:T(8,128)(2,1)S(1)} %get-tuple-element.46), channel_id=1, source_target_pairs={{0,3},{1,0},{2,1},{3,2},{4,7},{5,4},{6,5},{7,6},{8,11},{9,8},{10,9... | collective-permute-start | bytes 589832 | tf_op jit(solution)/shard_map/ppermute | solution.py:296
  30.2 0.2 all-to-all-done
  30.3 21.9 %all_gather.3.rows = bf16[8,384,128]{2,1,0:T(8,128)(2,1)S(1)} all-gather(bf16[1,384,128]{2,1,0:T(8,128)(2,1)S(1)} %bitcast.20), channel_id=1, replica_groups=mesh['z'=12,'c'=2,'y'=8,'x'=4] {'y'}, dimensions={0}, use_global_device_ids=true | all-gather | bytes 884736 | tf_op jit(solution)/shard_map/all_gather | solution.py:323
  52.2 0.0 collective-permute-done.w1
  52.2 0.0 collective-permute-done.1.w2
  52.2 0.0 collective-permute-done.2.w3
  52.2 0.7 shard_map.136
  53.0 11.7 %all_to_all.25.parts = bf16[4,192,384]{2,1,0:T(8,128)(2,1)S(1)} all-to-all(bf16[4,192,384]{2,1,0:T(8,128)(2,1)S(1)} %get-tuple-element.47), channel_id=1, replica_groups=mesh['z'=12,'c'=2,'y'=8,'x'=4] {'x'}, dimensions={0} | all-to-all | bytes 1179648 | tf_op jit(solution)/shard_map/all_to_all | solution.py:291
  64.6 0.2 shard_map.137
  64.8 9.8 %all_to_all.26.acts = bf16[4,200,384]{2,1,0:T(8,128)(2,1)S(1)} all-to-all(bf16[4,200,384]{2,1,0:T(8,128)(2,1)S(1)} %shard_map.137), channel_id=1, replica_groups=mesh['z'=12,'c'=2,'y'=8,'x'=4] {'x'}, dimensions={0} | all-to-all | bytes 1228800 | tf_op jit(solution)/shard_map/all_to_all | solution.py:291
  74.6 1.5 %shard_map.138 = (bf16[8,72,384]{2,1,0:T(8,128)(2,1)}, bf16[192,512]{1,0:T(8,128)(2,1)S(1)}, bf16[192,512]{1,0:T(8,128)(2,1)S(1)}, bf16[192,512]{1,0:T(8,128)(2,1)S(1)}, bf16[192,512]{1,0:T(8,128)(2,1)S(1)}) custom-call(s32[1]{0:T(128)} %bitcast.here, bf16[4,200,384]{2,1,0:T(8,128)(2,1)S(1)} %all_to_all.26.acts, bf16[192,512]{1,0:T(8,128)(2,1)S(1)} %get-tuple-element.43.w0, ...), custom_call_target="tpu_custom_call" | custom-call | tf_op jit(solution)/shard_map/pallas_call | solution.py:279
  76.1 5.2 %all-to-all-start.3 = ((bf16[8,72,384]{2,1,0:T(8,128)(2,1)}), bf16[8,72,384]{2,1,0:T(8,128)(2,1)S(1)}, u32[]{:S(2)}, u32[]{:S(2)}) async-start(bf16[8,72,384]{2,1,0:T(8,128)(2,1)} %get-tuple-element.50), calls=%async_computation.3 | async-start | bytes 884736 | tf_op jit(solution)/shard_map/all_to_all | solution.py:291
  81.3 2.2 %collective-permute-start.3 = (bf16[192,512]{1,0:T(8,128)(2,1)S(1)}, bf16[192,512]{1,0:T(8,128)(2,1)S(1)}, u32[]{:S(2)}, u32[]{:S(2)}) collective-permute-start(bf16[192,512]{1,0:T(8,128)(2,1)S(1)} %get-tuple-element.51), channel_id=1, source_target_pairs={{0,1},{1,2},{2,3},{3,0},{4,5},{5,6},{6,7},{7,4},{8,9},{9,10},{10,1... | collective-permute-start | bytes 589832 | tf_op jit(solution)/shard_map/ppermute | solution.py:296
  83.5 4.3 %collective-permute-start.4 = (bf16[192,512]{1,0:T(8,128)(2,1)S(1)}, bf16[192,512]{1,0:T(8,128)(2,1)S(1)}, u32[]{:S(2)}, u32[]{:S(2)}) collective-permute-start(bf16[192,512]{1,0:T(8,128)(2,1)S(1)} %get-tuple-element.52), channel_id=1, source_target_pairs={{0,3},{1,0},{2,1},{3,2},{4,7},{5,4},{6,5},{7,6},{8,11},{9,8},{10,9... | collective-permute-start | bytes 589832 | tf_op jit(solution)/shard_map/ppermute | solution.py:296
  87.8 1.1 collective-permute-done.3.p1
  89.0 1.5 %collective-permute-done.4.p3 = bf16[192,512]{1,0:T(8,128)(2,1)S(1)} collective-permute-done((bf16[192,512]{1,0:T(8,128)(2,1)S(1)}, bf16[192,512]{1,0:T(8,128)(2,1)S(1)}, u32[]{:S(2)}, u32[]{:S(2)}) %collective-permute-start.4) | collective-permute-done | bytes 196640 | tf_op jit(solution)/shard_map/ppermute | solution.py:296
  90.4 2.2 %all-to-all-done.3.parts = bf16[8,72,384]{2,1,0:T(8,128)(2,1)S(1)} async-done(((bf16[8,72,384]{2,1,0:T(8,128)(2,1)}), bf16[8,72,384]{2,1,0:T(8,128)(2,1)S(1)}, u32[]{:S(2)}, u32[]{:S(2)}) %all-to-all-start.3) | async-done | bytes 442400 | tf_op jit(solution)/shard_map/all_to_all | solution.py:291
  92.6 0.8 shard_map.139
  93.4 17.8 %all-to-all-start.4 = ((bf16[24,16,128]{2,1,0:T(8,128)(2,1)}), bf16[24,16,128]{2,1,0:T(8,128)(2,1)S(1)}, u32[]{:S(2)}, u32[]{:S(2)}) async-start(bf16[24,16,128]{2,1,0:T(8,128)(2,1)} %bitcast.10), calls=%async_computation.4 | async-start | bytes 196608 | tf_op jit(solution)/shard_map/all_to_all | solution.py:291
  111.2 2.6 %collective-permute-start.8 = (bf16[192,512]{1,0:T(8,128)(2,1)S(1)}, bf16[192,512]{1,0:T(8,128)(2,1)S(1)}, u32[]{:S(2)}, u32[]{:S(2)}) collective-permute-start(bf16[192,512]{1,0:T(8,128)(2,1)S(1)} %get-tuple-element.62), channel_id=1, source_target_pairs={{0,2},{1,3},{2,0},{3,1},{4,6},{5,7},{6,4},{7,5},{8,10},{9,11},{10,... | collective-permute-start | bytes 589832 | tf_op jit(solution)/shard_map/ppermute | solution.py:296
  113.8 3.9 %collective-permute-start.7 = (f32[8,128]{1,0:T(8,128)S(1)}, f32[8,128]{1,0:T(8,128)S(1)}, u32[]{:S(2)}, u32[]{:S(2)}) collective-permute-start(f32[8,128]{1,0:T(8,128)S(1)} %get-tuple-element.57.n0), channel_id=1, source_target_pairs={{0,3},{1,0},{2,1},{3,2},{4,7},{5,4},{6,5},{7,6},{8,11},{9,8},{10,9... | collective-permute-start | bytes 12296 | tf_op jit(solution)/shard_map/ppermute | solution.py:296
  117.7 2.8 %collective-permute-start.6 = (f32[8,128]{1,0:T(8,128)S(1)}, f32[8,128]{1,0:T(8,128)S(1)}, u32[]{:S(2)}, u32[]{:S(2)}) collective-permute-start(f32[8,128]{1,0:T(8,128)S(1)} %get-tuple-element.57.n0), channel_id=1, source_target_pairs={{0,2},{1,3},{2,0},{3,1},{4,6},{5,7},{6,4},{7,5},{8,10},{9,11},{10,... | collective-permute-start | bytes 12296 | tf_op jit(solution)/shard_map/ppermute | solution.py:296
  120.6 2.1 %collective-permute-start.5 = (f32[8,128]{1,0:T(8,128)S(1)}, f32[8,128]{1,0:T(8,128)S(1)}, u32[]{:S(2)}, u32[]{:S(2)}) collective-permute-start(f32[8,128]{1,0:T(8,128)S(1)} %get-tuple-element.57.n0), channel_id=1, source_target_pairs={{0,1},{1,2},{2,3},{3,0},{4,5},{5,6},{6,7},{7,4},{8,9},{9,10},{10,1... | collective-permute-start | bytes 12296 | tf_op jit(solution)/shard_map/ppermute | solution.py:296
  122.7 0.0 collective-permute-done.8.p2
  122.7 1.3 %shard_map.141 = (f32[64,2048]{1,0:T(8,128)}, f32[64,2048]{1,0:T(8,128)}, f32[64,2048]{1,0:T(8,128)}, f32[1,64]{1,0:T(1,128)}) custom-call(s32[1]{0:T(128)} %bitcast.here, bf16[192,512]{1,0:T(8,128)(2,1)S(1)} %get-tuple-element.60.p0, bf16[192,512]{1,0:T(8,128)(2,1)S(1)} %collective-permute-done.3.p1, bf16[192,512]{1,0:T(8,128)(2,1)S(1)} %collective-permute-done.8.p2, ...), custom_call_target="tpu_custom_call" | custom-call | tf_op jit(solution)/shard_map/pallas_call | solution.py:279
  124.1 0.0 collective-permute-done.7.n3
  124.1 0.0 collective-permute-done.6.n2
  124.1 2.0 %collective-permute-done.5.n1 = f32[8,128]{1,0:T(8,128)S(1)} collective-permute-done((f32[8,128]{1,0:T(8,128)S(1)}, f32[8,128]{1,0:T(8,128)S(1)}, u32[]{:S(2)}, u32[]{:S(2)}) %collective-permute-start.5) | collective-permute-done | bytes 4128 | tf_op jit(solution)/shard_map/ppermute | solution.py:296
  126.1 0.0 all-to-all-done.4
  126.1 0.8 shard_map.140
Async XLA Ops:
  2.6 27.7 %all-to-all-start = ((bf16[24,16,128]{2,1,0:T(8,128)(2,1)}), bf16[24,16,128]{2,1,0:T(8,128)(2,1)S(1)}, u32[]{:S(2)}, u32[]{:S(2)}) async-start(bf16[24,16,128]{2,1,0:T(8,128)(2,1)} %bitcast.8), calls=%async_computation | async-start | bytes 196608 | tf_op jit(solution)/shard_map/all_to_all | solution.py:291
  19.6 32.6 %collective-permute-start = (bf16[192,512]{1,0:T(8,128)(2,1)S(1)}, bf16[192,512]{1,0:T(8,128)(2,1)S(1)}, u32[]{:S(2)}, u32[]{:S(2)}) collective-permute-start(bf16[192,512]{1,0:T(8,128)(2,1)S(1)} %get-tuple-element.44), channel_id=1, source_target_pairs={{0,1},{1,2},{2,3},{3,0},{4,5},{5,6},{6,7},{7,4},{8,9},{9,10},{10,1... | collective-permute-start | bytes 589832 | tf_op jit(solution)/shard_map/ppermute | solution.py:296
  22.7 29.5 %collective-permute-start.1 = (bf16[192,512]{1,0:T(8,128)(2,1)S(1)}, bf16[192,512]{1,0:T(8,128)(2,1)S(1)}, u32[]{:S(2)}, u32[]{:S(2)}) collective-permute-start(bf16[192,512]{1,0:T(8,128)(2,1)S(1)} %get-tuple-element.45), channel_id=1, source_target_pairs={{0,2},{1,3},{2,0},{3,1},{4,6},{5,7},{6,4},{7,5},{8,10},{9,11},{10,... | collective-permute-start | bytes 589832 | tf_op jit(solution)/shard_map/ppermute | solution.py:296
  27.1 25.1 %collective-permute-start.2 = (bf16[192,512]{1,0:T(8,128)(2,1)S(1)}, bf16[192,512]{1,0:T(8,128)(2,1)S(1)}, u32[]{:S(2)}, u32[]{:S(2)}) collective-permute-start(bf16[192,512]{1,0:T(8,128)(2,1)S(1)} %get-tuple-element.46), channel_id=1, source_target_pairs={{0,3},{1,0},{2,1},{3,2},{4,7},{5,4},{6,5},{7,6},{8,11},{9,8},{10,9... | collective-permute-start | bytes 589832 | tf_op jit(solution)/shard_map/ppermute | solution.py:296
  76.1 16.5 %all-to-all-start.3 = ((bf16[8,72,384]{2,1,0:T(8,128)(2,1)}), bf16[8,72,384]{2,1,0:T(8,128)(2,1)S(1)}, u32[]{:S(2)}, u32[]{:S(2)}) async-start(bf16[8,72,384]{2,1,0:T(8,128)(2,1)} %get-tuple-element.50), calls=%async_computation.3 | async-start | bytes 884736 | tf_op jit(solution)/shard_map/all_to_all | solution.py:291
  81.3 7.6 %collective-permute-start.3 = (bf16[192,512]{1,0:T(8,128)(2,1)S(1)}, bf16[192,512]{1,0:T(8,128)(2,1)S(1)}, u32[]{:S(2)}, u32[]{:S(2)}) collective-permute-start(bf16[192,512]{1,0:T(8,128)(2,1)S(1)} %get-tuple-element.51), channel_id=1, source_target_pairs={{0,1},{1,2},{2,3},{3,0},{4,5},{5,6},{6,7},{7,4},{8,9},{9,10},{10,1... | collective-permute-start | bytes 589832 | tf_op jit(solution)/shard_map/ppermute | solution.py:296
  83.5 6.9 %collective-permute-start.4 = (bf16[192,512]{1,0:T(8,128)(2,1)S(1)}, bf16[192,512]{1,0:T(8,128)(2,1)S(1)}, u32[]{:S(2)}, u32[]{:S(2)}) collective-permute-start(bf16[192,512]{1,0:T(8,128)(2,1)S(1)} %get-tuple-element.52), channel_id=1, source_target_pairs={{0,3},{1,0},{2,1},{3,2},{4,7},{5,4},{6,5},{7,6},{8,11},{9,8},{10,9... | collective-permute-start | bytes 589832 | tf_op jit(solution)/shard_map/ppermute | solution.py:296
  93.4 32.7 %all-to-all-start.4 = ((bf16[24,16,128]{2,1,0:T(8,128)(2,1)}), bf16[24,16,128]{2,1,0:T(8,128)(2,1)S(1)}, u32[]{:S(2)}, u32[]{:S(2)}) async-start(bf16[24,16,128]{2,1,0:T(8,128)(2,1)} %bitcast.10), calls=%async_computation.4 | async-start | bytes 196608 | tf_op jit(solution)/shard_map/all_to_all | solution.py:291
  111.2 11.5 %collective-permute-start.8 = (bf16[192,512]{1,0:T(8,128)(2,1)S(1)}, bf16[192,512]{1,0:T(8,128)(2,1)S(1)}, u32[]{:S(2)}, u32[]{:S(2)}) collective-permute-start(bf16[192,512]{1,0:T(8,128)(2,1)S(1)} %get-tuple-element.62), channel_id=1, source_target_pairs={{0,2},{1,3},{2,0},{3,1},{4,6},{5,7},{6,4},{7,5},{8,10},{9,11},{10,... | collective-permute-start | bytes 589832 | tf_op jit(solution)/shard_map/ppermute | solution.py:296
  113.8 10.3 %collective-permute-start.7 = (f32[8,128]{1,0:T(8,128)S(1)}, f32[8,128]{1,0:T(8,128)S(1)}, u32[]{:S(2)}, u32[]{:S(2)}) collective-permute-start(f32[8,128]{1,0:T(8,128)S(1)} %get-tuple-element.57.n0), channel_id=1, source_target_pairs={{0,3},{1,0},{2,1},{3,2},{4,7},{5,4},{6,5},{7,6},{8,11},{9,8},{10,9... | collective-permute-start | bytes 12296 | tf_op jit(solution)/shard_map/ppermute | solution.py:296
  117.7 6.3 %collective-permute-start.6 = (f32[8,128]{1,0:T(8,128)S(1)}, f32[8,128]{1,0:T(8,128)S(1)}, u32[]{:S(2)}, u32[]{:S(2)}) collective-permute-start(f32[8,128]{1,0:T(8,128)S(1)} %get-tuple-element.57.n0), channel_id=1, source_target_pairs={{0,2},{1,3},{2,0},{3,1},{4,6},{5,7},{6,4},{7,5},{8,10},{9,11},{10,... | collective-permute-start | bytes 12296 | tf_op jit(solution)/shard_map/ppermute | solution.py:296
  120.6 5.6 %collective-permute-start.5 = (f32[8,128]{1,0:T(8,128)S(1)}, f32[8,128]{1,0:T(8,128)S(1)}, u32[]{:S(2)}, u32[]{:S(2)}) collective-permute-start(f32[8,128]{1,0:T(8,128)S(1)} %get-tuple-element.57.n0), channel_id=1, source_target_pairs={{0,1},{1,2},{2,3},{3,0},{4,5},{5,6},{6,7},{7,4},{8,9},{9,10},{10,1... | collective-permute-start | bytes 12296 | tf_op jit(solution)/shard_map/ppermute | solution.py:296
where the time goes:
time: 129 us; the launch traced here: 127 us
  starting transfers between devices  68.2 us (53%)
  blocking collectives  43.4 us (34%)
  Pallas kernels  7.61 us (6%)
  waiting for transfers between devices  6.98 us (5%)
    all_to_all x3, starting transfers between devices, swap(): return lax.all_to_all(a, axis, 0, 0, tiled=True)  39.7 us
    ppermute x9, starting transfers between devices, shifted(): return lax.ppermute(piece, axis, [(i, (i + d) % n) for i in range(n)])  28.5 us
    all_gather x1, blocking collectives, layer(): rows = lax.all_gather(mine, 'y', axis=0, tiled=False)  21.9 us
    all_to_all x2, blocking collectives, swap(): return lax.all_to_all(a, axis, 0, 0, tiled=True)  21.5 us
    pallas_call x8, Pallas kernels, call(): pl.pallas_call(body, out_shape=[shape(s, d) for s, d in outs], in_specs=s...  7.61 us
    ppermute x9, waiting for transfers between devices, shifted(): return lax.ppermute(piece, axis, [(i, (i + d) % n) for i in range(n)])  4.65 us
  transfers between devices with their start and end apart: 12, of which 5 were waited for; matrix products, arithmetic and copies ran while one was open for 0% of the time, Pallas kernels for 1%

commit v1 on v0

--- a/solution.py
+++ b/solution.py
@@ -116,9 +116,9 @@
 def partial_body(here, rows, w0, w1, w2, w3, out, x_out, s_out):
     weights = (w0, w1, w2, w3)
     nx = len(weights)
-    ny = rows.shape[0]
+    ny = rows.shape[1] // 128
     for j in range(ny // 2):
-        a, b = rows[2 * j], rows[2 * j + 1]
+        a, b = (rows[:, k * 128 : (k + 1) * 128] for k in (2 * j, 2 * j + 1))
         x_out[:, j * 128 : (j + 1) * 128] = jnp.concatenate([a[:, :HALF], b[:, :HALF]], axis=1)
         s_out[:, j * 128 : (j + 1) * 128] = jnp.concatenate([a[:, HALF:], b[:, HALF:]], axis=1)
     x, s = x_out[...], s_out[...]
@@ -151,8 +151,11 @@
         out[q] = block
 
 
-def backward_body(here, acts, w0, w1, w2, w3, x_rows, s_rows, back, *grads):
+def backward_body(
+    here, acts, w0, w1, w2, w3, x_rows, s_rows, back_far, g0, g1, g2, g3, back, sems
+):
     weights = (w0, w1, w2, w3)
+    grads = (g0, g1, g2, g3)
     nx, ny = len(weights), back.shape[0]
     hid = w0.shape[0] // 3
     width = w0.shape[1]
@@ -164,6 +167,14 @@
         0,
         0,
     ).astype(BF16)
+    for j in range(ny):
+        back[j, :HALF, :] = terms[j * HALF : (j + 1) * HALF]
+    ends = (slice(0, HALF), slice(HALF, back.shape[1]))
+    out_copies = [
+        pltpu.make_async_copy(back.at[:, e, :], back_far.at[:, e, :], sems.at[k])
+        for k, e in enumerate(ends)
+    ]
+    out_copies[0].start()
     hiddens = [acts[(here[0] + d) % nx, 2 * hid : 3 * hid, :] for d in range(nx)]
     pair = dot(jnp.concatenate(pairs, axis=0), x_rows[...], 1, 0)
     down = dot(jnp.concatenate(hiddens, axis=0), s_rows[...], 1, 0)
@@ -184,8 +195,10 @@
     lines += [flat[:, k : k + slots] for k in range(0, flat.shape[1], slots)]
     extra = jnp.concatenate(lines, axis=0)
     for j in range(ny):
-        back[j, :HALF, :] = terms[j * HALF : (j + 1) * HALF]
         back[j, HALF:, :] = extra
+    out_copies[1].start()
+    for c in out_copies:
+        c.wait()
 
 
 def gathered_body(parts, sent, norms):
@@ -269,18 +282,21 @@
         )
 
 
-def call(body, outs, *args, fetch=False, far=False, scratch=(), aliases=None):
+def call(body, outs, *args, fetch=False, far=False, scratch=(), aliases=None, sent=()):
     smem = pl.BlockSpec(memory_space=pltpu.SMEM)
     vmem = pl.BlockSpec(memory_space=pltpu.VMEM)
     space = pltpu.HBM if fetch else pltpu.VMEM
     specs = [smem if a.ndim == 1 else pl.BlockSpec(memory_space=space) for a in args]
     args = [a if a.ndim == 1 else pltpu.with_memory_space_constraint(a, space) for a in args]
     shape = jax.ShapeDtypeStruct if far else pltpu.VMEM
+    shapes = [pltpu.HBM(a, d) if k in sent else shape(a, d) for k, (a, d) in enumerate(outs)]
     return pl.pallas_call(
         body,
-        out_shape=[shape(s, d) for s, d in outs],
+        out_shape=shapes,
         in_specs=specs,
-        out_specs=[vmem] * len(outs),
+        out_specs=[
+            pl.BlockSpec(memory_space=pltpu.HBM) if k in sent else vmem for k in range(len(outs))
+        ],
         scratch_shapes=list(scratch),
         input_output_aliases=aliases or {},
         compiler_params=pltpu.CompilerParams(vmem_limit_bytes=ROOM),
@@ -320,7 +336,7 @@
     w_sent = call(quarter_weights_body, [((3 * hid, quarter), BF16)] * nx, here, *local)
     mine = swap(sent.reshape(sources, SLOTS, 2 * feat), ("z", "c")).reshape(slots, 2 * feat)
     weights = [w_sent[0]] + [shifted(w_sent[d], "x", d) for d in range(1, nx)]
-    rows = lax.all_gather(mine, "y", axis=0, tiled=False)
+    rows = lax.all_gather(mine, "y", axis=1, tiled=True)
     parts, x_rows, s_rows = call(
         partial_body,
         [
@@ -344,6 +360,8 @@
         *weights,
         x_rows,
         s_rows,
+        sent=(0,),
+        scratch=[pltpu.VMEM((ny, feat + 8, slots), BF16), pltpu.SemaphoreType.DMA((2,))],
     )
     grads = [grads[0]] + [shifted(grads[d], "x", d) for d in range(1, nx)]
     back = swap(back, "y")

time: 129 us -> 127 us (0.984)
  starting transfers between devices: 68.2 us -> 65.4 us
    all_to_all x3, starting transfers between devices: 39.7 us -> 36.9 us  [swap(): return lax.all_to_all(a, axis, 0, 0, tiled=True)]
    all_gather x1, blocking collectives: 21.9 us -> 24.1 us  [layer(): rows = lax.all_gather(mine, 'y', axis=1, tiled=True)]
where the time goes in v1:
time: 127 us; the launch traced here: 125 us
  starting transfers between devices  65.4 us (51%)
  blocking collectives  44.6 us (35%)
  Pallas kernels  7.47 us (6%)
  waiting for transfers between devices  6.98 us (5%)
    all_to_all x3, starting transfers between devices, swap(): return lax.all_to_all(a, axis, 0, 0, tiled=True)  36.9 us
    ppermute x9, starting transfers between devices, shifted(): return lax.ppermute(piece, axis, [(i, (i + d) % n) for i in range(n)])  28.5 us
    all_gather x1, blocking collectives, layer(): rows = lax.all_gather(mine, 'y', axis=1, tiled=True)  24.1 us
    all_to_all x2, blocking collectives, swap(): return lax.all_to_all(a, axis, 0, 0, tiled=True)  20.5 us
    pallas_call x8, Pallas kernels, call(): pl.pallas_call(body, out_shape=shapes, in_specs=specs, out_specs=[pl.Bloc...  7.47 us
    ppermute x9, waiting for transfers between devices, shifted(): return lax.ppermute(piece, axis, [(i, (i + d) % n) for i in range(n)])  4.65 us
  transfers between devices with their start and end apart: 12, of which 5 were waited for; matrix products, arithmetic and copies ran while one was open for 0% of the time, Pallas kernels for 1%

profile of v1, /device:TPU:1, one launch (start us, length us, event | category | flops | bytes accessed | tf_op | source)
XLA Modules:
  0.0 125.2 jit_solution(11911315198702869342)
XLA Ops:
  0.6 2.0 %shard_map.134 = (bf16[384,128]{1,0:T(8,128)(2,1)}, s32[2,128]{1,0:T(2,128)S(1)}, f32[2,128]{1,0:T(2,128)S(1)}, bf16[64,2048]{1,0:T(8,128)(2,1)S(1)}, bf16[64,20...) custom-call(bf16[64,128]{1,0:T(8,128)(2,1)} %bitcast.24, s32[2,128]{1,0:T(2,128)} %bitcast.26, f32[2,128]{1,0:T(2,128)} %bitcast.27, ...), custom_call_target="tpu_custom_call" | custom-call | tf_op jit(solution)/shard_map/pallas_call | solution.py:293
  2.6 16.7 %all-to-all-start = ((bf16[24,16,128]{2,1,0:T(8,128)(2,1)}), bf16[24,16,128]{2,1,0:T(8,128)(2,1)S(1)}, u32[]{:S(2)}, u32[]{:S(2)}) async-start(bf16[24,16,128]{2,1,0:T(8,128)(2,1)} %bitcast.8), calls=%async_computation | async-start | bytes 196608 | tf_op jit(solution)/shard_map/all_to_all | solution.py:307
  19.3 0.3 shard_map.135
  19.6 3.1 %collective-permute-start = (bf16[192,512]{1,0:T(8,128)(2,1)S(1)}, bf16[192,512]{1,0:T(8,128)(2,1)S(1)}, u32[]{:S(2)}, u32[]{:S(2)}) collective-permute-start(bf16[192,512]{1,0:T(8,128)(2,1)S(1)} %get-tuple-element.44), channel_id=1, source_target_pairs={{0,1},{1,2},{2,3},{3,0},{4,5},{5,6},{6,7},{7,4},{8,9},{9,10},{10,1... | collective-permute-start | bytes 589832 | tf_op jit(solution)/shard_map/ppermute | solution.py:312
  22.7 4.4 %collective-permute-start.1 = (bf16[192,512]{1,0:T(8,128)(2,1)S(1)}, bf16[192,512]{1,0:T(8,128)(2,1)S(1)}, u32[]{:S(2)}, u32[]{:S(2)}) collective-permute-start(bf16[192,512]{1,0:T(8,128)(2,1)S(1)} %get-tuple-element.45), channel_id=1, source_target_pairs={{0,2},{1,3},{2,0},{3,1},{4,6},{5,7},{6,4},{7,5},{8,10},{9,11},{10,... | collective-permute-start | bytes 589832 | tf_op jit(solution)/shard_map/ppermute | solution.py:312
  27.1 3.1 %collective-permute-start.2 = (bf16[192,512]{1,0:T(8,128)(2,1)S(1)}, bf16[192,512]{1,0:T(8,128)(2,1)S(1)}, u32[]{:S(2)}, u32[]{:S(2)}) collective-permute-start(bf16[192,512]{1,0:T(8,128)(2,1)S(1)} %get-tuple-element.46), channel_id=1, source_target_pairs={{0,3},{1,0},{2,1},{3,2},{4,7},{5,4},{6,5},{7,6},{8,11},{9,8},{10,9... | collective-permute-start | bytes 589832 | tf_op jit(solution)/shard_map/ppermute | solution.py:312
  30.2 0.2 all-to-all-done
  30.3 24.1 %all_gather.3.rows = bf16[384,1024]{1,0:T(8,128)(2,1)S(1)} all-gather(bf16[384,128]{1,0:T(8,128)(2,1)S(1)} %bitcast.20), channel_id=1, replica_groups=mesh['z'=12,'c'=2,'y'=8,'x'=4] {'y'}, dimensions={1}, use_global_device_ids=true | all-gather | bytes 884736 | tf_op jit(solution)/shard_map/all_gather | solution.py:339
  54.4 0.0 collective-permute-done.w1
  54.4 0.0 collective-permute-done.1.w2
  54.4 0.0 collective-permute-done.2.w3
  54.4 0.7 shard_map.136
  55.1 10.7 %all_to_all.25.parts = bf16[4,192,384]{2,1,0:T(8,128)(2,1)S(1)} all-to-all(bf16[4,192,384]{2,1,0:T(8,128)(2,1)S(1)} %get-tuple-element.47), channel_id=1, replica_groups=mesh['z'=12,'c'=2,'y'=8,'x'=4] {'x'}, dimensions={0} | all-to-all | bytes 1179648 | tf_op jit(solution)/shard_map/all_to_all | solution.py:307
  65.8 0.2 shard_map.137
  66.0 9.8 %all_to_all.26.acts = bf16[4,200,384]{2,1,0:T(8,128)(2,1)S(1)} all-to-all(bf16[4,200,384]{2,1,0:T(8,128)(2,1)S(1)} %shard_map.137), channel_id=1, replica_groups=mesh['z'=12,'c'=2,'y'=8,'x'=4] {'x'}, dimensions={0} | all-to-all | bytes 1228800 | tf_op jit(solution)/shard_map/all_to_all | solution.py:307
  75.8 1.4 %shard_map.138 = (bf16[8,72,384]{2,1,0:T(8,128)(2,1)}, bf16[192,512]{1,0:T(8,128)(2,1)S(1)}, bf16[192,512]{1,0:T(8,128)(2,1)S(1)}, bf16[192,512]{1,0:T(8,128)(2,1)S(1)}, bf16[192,512]{1,0:T(8,128)(2,1)S(1)}) custom-call(s32[1]{0:T(128)} %bitcast.here, bf16[4,200,384]{2,1,0:T(8,128)(2,1)S(1)} %all_to_all.26.acts, bf16[192,512]{1,0:T(8,128)(2,1)S(1)} %get-tuple-element.43.w0, ...), custom_call_target="tpu_custom_call" | custom-call | tf_op jit(solution)/shard_map/pallas_call | solution.py:293
  77.2 3.8 %all-to-all-start.3 = ((bf16[8,72,384]{2,1,0:T(8,128)(2,1)}), bf16[8,72,384]{2,1,0:T(8,128)(2,1)S(1)}, u32[]{:S(2)}, u32[]{:S(2)}) async-start(bf16[8,72,384]{2,1,0:T(8,128)(2,1)} %get-tuple-element.50), calls=%async_computation.3 | async-start | bytes 884736 | tf_op jit(solution)/shard_map/all_to_all | solution.py:307
  81.0 2.2 %collective-permute-start.3 = (bf16[192,512]{1,0:T(8,128)(2,1)S(1)}, bf16[192,512]{1,0:T(8,128)(2,1)S(1)}, u32[]{:S(2)}, u32[]{:S(2)}) collective-permute-start(bf16[192,512]{1,0:T(8,128)(2,1)S(1)} %get-tuple-element.51), channel_id=1, source_target_pairs={{0,1},{1,2},{2,3},{3,0},{4,5},{5,6},{6,7},{7,4},{8,9},{9,10},{10,1... | collective-permute-start | bytes 589832 | tf_op jit(solution)/shard_map/ppermute | solution.py:312
  83.2 4.3 %collective-permute-start.4 = (bf16[192,512]{1,0:T(8,128)(2,1)S(1)}, bf16[192,512]{1,0:T(8,128)(2,1)S(1)}, u32[]{:S(2)}, u32[]{:S(2)}) collective-permute-start(bf16[192,512]{1,0:T(8,128)(2,1)S(1)} %get-tuple-element.52), channel_id=1, source_target_pairs={{0,3},{1,0},{2,1},{3,2},{4,7},{5,4},{6,5},{7,6},{8,11},{9,8},{10,9... | collective-permute-start | bytes 589832 | tf_op jit(solution)/shard_map/ppermute | solution.py:312
  87.5 1.1 collective-permute-done.3.p1
  88.7 1.5 %collective-permute-done.4.p3 = bf16[192,512]{1,0:T(8,128)(2,1)S(1)} collective-permute-done((bf16[192,512]{1,0:T(8,128)(2,1)S(1)}, bf16[192,512]{1,0:T(8,128)(2,1)S(1)}, u32[]{:S(2)}, u32[]{:S(2)}) %collective-permute-start.4) | collective-permute-done | bytes 196640 | tf_op jit(solution)/shard_map/ppermute | solution.py:312
  90.1 2.2 %all-to-all-done.3.parts = bf16[8,72,384]{2,1,0:T(8,128)(2,1)S(1)} async-done(((bf16[8,72,384]{2,1,0:T(8,128)(2,1)}), bf16[8,72,384]{2,1,0:T(8,128)(2,1)S(1)}, u32[]{:S(2)}, u32[]{:S(2)}) %all-to-all-start.3) | async-done | bytes 442400 | tf_op jit(solution)/shard_map/all_to_all | solution.py:307
  92.3 0.8 shard_map.139
  93.1 16.4 %all-to-all-start.4 = ((bf16[24,16,128]{2,1,0:T(8,128)(2,1)}), bf16[24,16,128]{2,1,0:T(8,128)(2,1)S(1)}, u32[]{:S(2)}, u32[]{:S(2)}) async-start(bf16[24,16,128]{2,1,0:T(8,128)(2,1)} %bitcast.10), calls=%async_computation.4 | async-start | bytes 196608 | tf_op jit(solution)/shard_map/all_to_all | solution.py:307
  109.5 2.6 %collective-permute-start.8 = (bf16[192,512]{1,0:T(8,128)(2,1)S(1)}, bf16[192,512]{1,0:T(8,128)(2,1)S(1)}, u32[]{:S(2)}, u32[]{:S(2)}) collective-permute-start(bf16[192,512]{1,0:T(8,128)(2,1)S(1)} %get-tuple-element.62), channel_id=1, source_target_pairs={{0,2},{1,3},{2,0},{3,1},{4,6},{5,7},{6,4},{7,5},{8,10},{9,11},{10,... | collective-permute-start | bytes 589832 | tf_op jit(solution)/shard_map/ppermute | solution.py:312
  112.1 3.9 %collective-permute-start.7 = (f32[8,128]{1,0:T(8,128)S(1)}, f32[8,128]{1,0:T(8,128)S(1)}, u32[]{:S(2)}, u32[]{:S(2)}) collective-permute-start(f32[8,128]{1,0:T(8,128)S(1)} %get-tuple-element.57.n0), channel_id=1, source_target_pairs={{0,3},{1,0},{2,1},{3,2},{4,7},{5,4},{6,5},{7,6},{8,11},{9,8},{10,9... | collective-permute-start | bytes 12296 | tf_op jit(solution)/shard_map/ppermute | solution.py:312
  116.0 2.8 %collective-permute-start.6 = (f32[8,128]{1,0:T(8,128)S(1)}, f32[8,128]{1,0:T(8,128)S(1)}, u32[]{:S(2)}, u32[]{:S(2)}) collective-permute-start(f32[8,128]{1,0:T(8,128)S(1)} %get-tuple-element.57.n0), channel_id=1, source_target_pairs={{0,2},{1,3},{2,0},{3,1},{4,6},{5,7},{6,4},{7,5},{8,10},{9,11},{10,... | collective-permute-start | bytes 12296 | tf_op jit(solution)/shard_map/ppermute | solution.py:312
  118.8 2.1 %collective-permute-start.5 = (f32[8,128]{1,0:T(8,128)S(1)}, f32[8,128]{1,0:T(8,128)S(1)}, u32[]{:S(2)}, u32[]{:S(2)}) collective-permute-start(f32[8,128]{1,0:T(8,128)S(1)} %get-tuple-element.57.n0), channel_id=1, source_target_pairs={{0,1},{1,2},{2,3},{3,0},{4,5},{5,6},{6,7},{7,4},{8,9},{9,10},{10,1... | collective-permute-start | bytes 12296 | tf_op jit(solution)/shard_map/ppermute | solution.py:312
  121.0 0.0 collective-permute-done.8.p2
  121.0 1.3 %shard_map.141 = (f32[64,2048]{1,0:T(8,128)}, f32[64,2048]{1,0:T(8,128)}, f32[64,2048]{1,0:T(8,128)}, f32[1,64]{1,0:T(1,128)}) custom-call(s32[1]{0:T(128)} %bitcast.here, bf16[192,512]{1,0:T(8,128)(2,1)S(1)} %get-tuple-element.60.p0, bf16[192,512]{1,0:T(8,128)(2,1)S(1)} %collective-permute-done.3.p1, bf16[192,512]{1,0:T(8,128)(2,1)S(1)} %collective-permute-done.8.p2, ...), custom_call_target="tpu_custom_call" | custom-call | tf_op jit(solution)/shard_map/pallas_call | solution.py:293
  122.3 0.0 collective-permute-done.7.n3
  122.3 0.0 collective-permute-done.6.n2
  122.3 2.0 %collective-permute-done.5.n1 = f32[8,128]{1,0:T(8,128)S(1)} collective-permute-done((f32[8,128]{1,0:T(8,128)S(1)}, f32[8,128]{1,0:T(8,128)S(1)}, u32[]{:S(2)}, u32[]{:S(2)}) %collective-permute-start.5) | collective-permute-done | bytes 4128 | tf_op jit(solution)/shard_map/ppermute | solution.py:312
  124.4 0.0 all-to-all-done.4
  124.4 0.8 shard_map.140
Async XLA Ops:
  2.6 27.7 %all-to-all-start = ((bf16[24,16,128]{2,1,0:T(8,128)(2,1)}), bf16[24,16,128]{2,1,0:T(8,128)(2,1)S(1)}, u32[]{:S(2)}, u32[]{:S(2)}) async-start(bf16[24,16,128]{2,1,0:T(8,128)(2,1)} %bitcast.8), calls=%async_computation | async-start | bytes 196608 | tf_op jit(solution)/shard_map/all_to_all | solution.py:307
  19.6 34.8 %collective-permute-start = (bf16[192,512]{1,0:T(8,128)(2,1)S(1)}, bf16[192,512]{1,0:T(8,128)(2,1)S(1)}, u32[]{:S(2)}, u32[]{:S(2)}) collective-permute-start(bf16[192,512]{1,0:T(8,128)(2,1)S(1)} %get-tuple-element.44), channel_id=1, source_target_pairs={{0,1},{1,2},{2,3},{3,0},{4,5},{5,6},{6,7},{7,4},{8,9},{9,10},{10,1... | collective-permute-start | bytes 589832 | tf_op jit(solution)/shard_map/ppermute | solution.py:312
  22.7 31.7 %collective-permute-start.1 = (bf16[192,512]{1,0:T(8,128)(2,1)S(1)}, bf16[192,512]{1,0:T(8,128)(2,1)S(1)}, u32[]{:S(2)}, u32[]{:S(2)}) collective-permute-start(bf16[192,512]{1,0:T(8,128)(2,1)S(1)} %get-tuple-element.45), channel_id=1, source_target_pairs={{0,2},{1,3},{2,0},{3,1},{4,6},{5,7},{6,4},{7,5},{8,10},{9,11},{10,... | collective-permute-start | bytes 589832 | tf_op jit(solution)/shard_map/ppermute | solution.py:312
  27.1 27.3 %collective-permute-start.2 = (bf16[192,512]{1,0:T(8,128)(2,1)S(1)}, bf16[192,512]{1,0:T(8,128)(2,1)S(1)}, u32[]{:S(2)}, u32[]{:S(2)}) collective-permute-start(bf16[192,512]{1,0:T(8,128)(2,1)S(1)} %get-tuple-element.46), channel_id=1, source_target_pairs={{0,3},{1,0},{2,1},{3,2},{4,7},{5,4},{6,5},{7,6},{8,11},{9,8},{10,9... | collective-permute-start | bytes 589832 | tf_op jit(solution)/shard_map/ppermute | solution.py:312
  77.2 15.1 %all-to-all-start.3 = ((bf16[8,72,384]{2,1,0:T(8,128)(2,1)}), bf16[8,72,384]{2,1,0:T(8,128)(2,1)S(1)}, u32[]{:S(2)}, u32[]{:S(2)}) async-start(bf16[8,72,384]{2,1,0:T(8,128)(2,1)} %get-tuple-element.50), calls=%async_computation.3 | async-start | bytes 884736 | tf_op jit(solution)/shard_map/all_to_all | solution.py:307
  81.0 7.6 %collective-permute-start.3 = (bf16[192,512]{1,0:T(8,128)(2,1)S(1)}, bf16[192,512]{1,0:T(8,128)(2,1)S(1)}, u32[]{:S(2)}, u32[]{:S(2)}) collective-permute-start(bf16[192,512]{1,0:T(8,128)(2,1)S(1)} %get-tuple-element.51), channel_id=1, source_target_pairs={{0,1},{1,2},{2,3},{3,0},{4,5},{5,6},{6,7},{7,4},{8,9},{9,10},{10,1... | collective-permute-start | bytes 589832 | tf_op jit(solution)/shard_map/ppermute | solution.py:312
  83.2 6.9 %collective-permute-start.4 = (bf16[192,512]{1,0:T(8,128)(2,1)S(1)}, bf16[192,512]{1,0:T(8,128)(2,1)S(1)}, u32[]{:S(2)}, u32[]{:S(2)}) collective-permute-start(bf16[192,512]{1,0:T(8,128)(2,1)S(1)} %get-tuple-element.52), channel_id=1, source_target_pairs={{0,3},{1,0},{2,1},{3,2},{4,7},{5,4},{6,5},{7,6},{8,11},{9,8},{10,9... | collective-permute-start | bytes 589832 | tf_op jit(solution)/shard_map/ppermute | solution.py:312
  93.1 31.3 %all-to-all-start.4 = ((bf16[24,16,128]{2,1,0:T(8,128)(2,1)}), bf16[24,16,128]{2,1,0:T(8,128)(2,1)S(1)}, u32[]{:S(2)}, u32[]{:S(2)}) async-start(bf16[24,16,128]{2,1,0:T(8,128)(2,1)} %bitcast.10), calls=%async_computation.4 | async-start | bytes 196608 | tf_op jit(solution)/shard_map/all_to_all | solution.py:307
  109.5 11.5 %collective-permute-start.8 = (bf16[192,512]{1,0:T(8,128)(2,1)S(1)}, bf16[192,512]{1,0:T(8,128)(2,1)S(1)}, u32[]{:S(2)}, u32[]{:S(2)}) collective-permute-start(bf16[192,512]{1,0:T(8,128)(2,1)S(1)} %get-tuple-element.62), channel_id=1, source_target_pairs={{0,2},{1,3},{2,0},{3,1},{4,6},{5,7},{6,4},{7,5},{8,10},{9,11},{10,... | collective-permute-start | bytes 589832 | tf_op jit(solution)/shard_map/ppermute | solution.py:312
  112.1 10.3 %collective-permute-start.7 = (f32[8,128]{1,0:T(8,128)S(1)}, f32[8,128]{1,0:T(8,128)S(1)}, u32[]{:S(2)}, u32[]{:S(2)}) collective-permute-start(f32[8,128]{1,0:T(8,128)S(1)} %get-tuple-element.57.n0), channel_id=1, source_target_pairs={{0,3},{1,0},{2,1},{3,2},{4,7},{5,4},{6,5},{7,6},{8,11},{9,8},{10,9... | collective-permute-start | bytes 12296 | tf_op jit(solution)/shard_map/ppermute | solution.py:312
  116.0 6.3 %collective-permute-start.6 = (f32[8,128]{1,0:T(8,128)S(1)}, f32[8,128]{1,0:T(8,128)S(1)}, u32[]{:S(2)}, u32[]{:S(2)}) collective-permute-start(f32[8,128]{1,0:T(8,128)S(1)} %get-tuple-element.57.n0), channel_id=1, source_target_pairs={{0,2},{1,3},{2,0},{3,1},{4,6},{5,7},{6,4},{7,5},{8,10},{9,11},{10,... | collective-permute-start | bytes 12296 | tf_op jit(solution)/shard_map/ppermute | solution.py:312
  118.8 5.6 %collective-permute-start.5 = (f32[8,128]{1,0:T(8,128)S(1)}, f32[8,128]{1,0:T(8,128)S(1)}, u32[]{:S(2)}, u32[]{:S(2)}) collective-permute-start(f32[8,128]{1,0:T(8,128)S(1)} %get-tuple-element.57.n0), channel_id=1, source_target_pairs={{0,1},{1,2},{2,3},{3,0},{4,5},{5,6},{6,7},{7,4},{8,9},{9,10},{10,1... | collective-permute-start | bytes 12296 | tf_op jit(solution)/shard_map/ppermute | solution.py:312
